TPU v7x, 32 devices: a whole 2x2x4 slice. The times are simulated.
32 devices in a mesh: sp: 8 (over z, x), tp: 4 (over y, core).
Axes of the slice: x: 2, y: 2, z: 4, core: 2. Of those that a mesh axis runs over, the one named last changes fastest.
Arguments:
- moe_input: bfloat16 [2048, 2048], P('sp'), may hold values from -6 to 6
- cotangent: bfloat16 [2048, 2048], P('sp'), may hold values from -6 to 6
- expert_ids: int32 [2048, 2], P('sp'), may hold values from 0 to 7, as said below
- route_weights: float32 [2048, 2], P('sp'), may hold values from 0.05 to 1
- gate_weight: bfloat16 [8, 2048, 1024], P('sp', None, 'tp'), may hold values from -0.125 to 0.125
- up_weight: bfloat16 [8, 2048, 1024], P('sp', None, 'tp'), may hold values from -0.125 to 0.125
- down_weight: bfloat16 [8, 1024, 2048], P('sp', 'tp'), may hold values from -0.1875 to 0.1875
- out_weight: bfloat16 [2048, 1024], P(None, 'tp'), may hold values from -0.1875 to 0.1875
- mixer_out: bfloat16 [2048, 1024], P('sp', 'tp'), may hold values from -6 to 6
- query_vectors: bfloat16 [2048, 512], P('sp', 'tp'), may hold values from -0.62109375 to 0.62109375
- key_vectors: bfloat16 [2048, 512], P('sp', 'tp'), may hold values from -0.62109375 to 0.62109375
- value_vectors: bfloat16 [2048, 1024], P('sp', 'tp'), may hold values from -6 to 6
- log_decay: float32 [2048, 512], P('sp', 'tp'), may hold values from -2 to 0
Outputs:
- grad_gate: bfloat16 [8, 2048, 1024], P('sp', None, 'tp')
- grad_up: bfloat16 [8, 2048, 1024], P('sp', None, 'tp')
- grad_down: bfloat16 [8, 1024, 2048], P('sp', 'tp')
- grad_out_weight: float32 [2048, 1024], P('sp', 'tp')
- grad_queries: bfloat16 [2048, 512], P('sp', 'tp')
- grad_keys: bfloat16 [2048, 512], P('sp', 'tp')
- grad_values: bfloat16 [2048, 1024], P('sp', 'tp')
- grad_log_decay: float32 [2048, 512], P('sp', 'tp')
Inputs may be any that keep to these rules, and one draw needn't show every extreme that they name: `expert_ids`: each row names two different experts of one group, expert e lying in group e // 2. Each aligned block of 256 rows names every expert exactly 64 times and has equally many rows in each of the 4 groups.
All inputs are finite; a program needn't handle non-finite values.
Results may differ from a plain program's by a relative error of at most 0.01145.
Values may be sent and summed in bfloat16 or wider, within the bound.
A program may use at most 64 MiB of HBM per device.

v0:
```python
import jax
import jax.numpy as jnp
from jax import lax
from jax.sharding import PartitionSpec as P

KEY_CHANNELS = 64
VAL_DIM = 128
BLOCK = 64
HIGHEST = lax.Precision.HIGHEST


def entering(shard, axis, combine, identity, reverse):
    devices, place = (lax.axis_size(axis), lax.axis_index(axis))
    everything = jax.tree.map(lambda part: lax.all_gather(part, axis), shard)
    start = jax.tree.map(
        lambda part, zero: jnp.broadcast_to(jnp.asarray(zero, part.dtype), part.shape),
        shard,
        identity,
    )

    def lap(k, before):
        at = devices - 1 - k if reverse else k
        reached = at > place if reverse else at < place
        new = combine(before, jax.tree.map(lambda part: part[at], everything))
        return jax.tree.map(lambda a, b: jnp.where(reached, a, b), new, before)

    return lax.fori_loop(0, devices, lap, start)


def block_step(memory, inputs):
    query_block, key_block, value_block, decay_block = inputs
    block_len = query_block.shape[1]
    causal = jnp.tril(jnp.ones((block_len, block_len), dtype=bool))
    cumulative = jnp.cumsum(decay_block, axis=1)
    carried = jnp.einsum(
        "hcd,hdv->hcv", query_block * jnp.exp(cumulative), memory, precision=HIGHEST
    )
    difference = cumulative[:, :, None, :] - cumulative[:, None, :, :]
    decay = jnp.exp(jnp.where(causal[None, :, :, None], difference, -jnp.inf))
    scores = jnp.einsum("htd,hsd,htsd->hts", query_block, key_block, decay, precision=HIGHEST)
    within = jnp.einsum("hts,hsv->htv", scores, value_block, precision=HIGHEST)
    final_row = cumulative[:, -1:, :]
    memory = jnp.exp(final_row[:, 0, :])[:, :, None] * memory + jnp.einsum(
        "hsd,hsv->hdv", key_block * jnp.exp(final_row - cumulative), value_block, precision=HIGHEST
    )
    return (memory, carried + within)


def run_blocks(query_heads, key_heads, value_heads, decay_heads, memory):
    head_count = query_heads.shape[0]
    length = query_heads.shape[1]
    block_count = length // BLOCK

    def to_blocks(matrix):
        return matrix.reshape(head_count, block_count, BLOCK, matrix.shape[-1]).transpose(
            1, 0, 2, 3
        )

    memory, outputs = lax.scan(
        jax.checkpoint(block_step),
        memory,
        (
            to_blocks(query_heads),
            to_blocks(key_heads),
            to_blocks(value_heads),
            to_blocks(decay_heads),
        ),
    )
    return (outputs.transpose(1, 0, 2, 3).reshape(head_count, length, outputs.shape[-1]), memory)


def chain_combine(former, latter):
    return (former[0] * latter[0], latter[1] + latter[0][:, :, None] * former[1])


def expert_pass(routed, routed_cot, gate_local, up_local, down_local):
    pre_gate = jnp.dot(routed, gate_local, preferred_element_type=jnp.float32)
    pre_up = jnp.dot(routed, up_local, preferred_element_type=jnp.float32)
    sigmoid_gate = jax.nn.sigmoid(pre_gate)
    activated = pre_gate * sigmoid_gate
    hidden = (activated * pre_up).astype(jnp.bfloat16)
    delta_hidden = jnp.dot(routed_cot, down_local.T, preferred_element_type=jnp.float32)
    grad_down = jnp.dot(hidden.T, routed_cot, preferred_element_type=jnp.float32).astype(
        jnp.bfloat16
    )
    delta_gate = (
        delta_hidden * pre_up * sigmoid_gate * (1.0 + pre_gate * (1.0 - sigmoid_gate))
    ).astype(jnp.bfloat16)
    delta_up = (delta_hidden * activated).astype(jnp.bfloat16)
    grad_gate = jnp.dot(routed.T, delta_gate, preferred_element_type=jnp.float32).astype(
        jnp.bfloat16
    )
    grad_up = jnp.dot(routed.T, delta_up, preferred_element_type=jnp.float32).astype(jnp.bfloat16)
    partial_value = jnp.dot(delta_gate, gate_local.T, preferred_element_type=jnp.float32)
    partial_value = partial_value + jnp.dot(
        delta_up, up_local.T, preferred_element_type=jnp.float32
    )
    return (grad_gate, grad_up, grad_down, partial_value)


def mixer_backward(query_vectors, key_vectors, value_vectors, log_decay, delta_mixer):
    tok_count = query_vectors.shape[0]

    def heads_first(matrix, channel_size):
        return matrix.astype(jnp.float32).reshape(tok_count, -1, channel_size).transpose(1, 0, 2)

    def tokens_first(matrix):
        return matrix.transpose(1, 0, 2).reshape(tok_count, -1)

    query_heads = heads_first(query_vectors, KEY_CHANNELS)
    key_heads = heads_first(key_vectors, KEY_CHANNELS)
    value_heads = heads_first(value_vectors, VAL_DIM)
    decay_heads = heads_first(log_decay, KEY_CHANNELS)
    cot_heads = heads_first(delta_mixer, VAL_DIM)
    cumulative = jnp.cumsum(decay_heads, axis=1)
    decay_total = cumulative[:, -1, :]
    retention = jnp.exp(decay_total)
    local_state = jnp.einsum(
        "hld,hlv->hdv",
        key_heads * jnp.exp(decay_total[:, None, :] - cumulative),
        value_heads,
        precision=HIGHEST,
    )
    local_pull = jnp.einsum(
        "hld,hlv->hdv",
        query_heads * KEY_CHANNELS ** (-0.5) * jnp.exp(cumulative),
        cot_heads,
        precision=HIGHEST,
    )
    identity = (jnp.ones_like(retention), jnp.zeros_like(local_state))
    start_state = entering((retention, local_state), "sp", chain_combine, identity, False)[1]
    end_pull = entering((retention, local_pull), "sp", chain_combine, identity, True)[1]

    def local_forward(query_in, key_in, value_in, decay_in):
        return run_blocks(
            query_in * KEY_CHANNELS ** (-0.5), key_in, value_in, decay_in, start_state
        )

    pullback = jax.vjp(local_forward, query_heads, key_heads, value_heads, decay_heads)[1]
    grads = pullback((cot_heads, end_pull))
    return (
        tokens_first(grads[0]).astype(jnp.bfloat16),
        tokens_first(grads[1]).astype(jnp.bfloat16),
        tokens_first(grads[2]).astype(jnp.bfloat16),
        tokens_first(grads[3]),
    )


def shards(
    moe_input,
    cotangent,
    expert_ids,
    route_weights,
    gate_weight,
    up_weight,
    down_weight,
    out_weight,
    mixer_out,
    query_vectors,
    key_vectors,
    value_vectors,
    log_decay,
):
    tok_count = moe_input.shape[0]
    model_width = moe_input.shape[1]
    slot_total = 2 * tok_count
    flat_ids = expert_ids.reshape(-1)
    sorting = jnp.argsort(flat_ids, stable=True)
    source_rows = sorting // 2
    inverse = jnp.argsort(sorting)
    gate_local = gate_weight[0]
    up_local = up_weight[0]
    down_local = down_weight[0]
    quarter = model_width // lax.axis_size("tp")
    offset = lax.axis_index("tp") * quarter
    own_input = lax.dynamic_slice_in_dim(moe_input, offset, quarter, 1)
    own_cot = lax.dynamic_slice_in_dim(cotangent, offset, quarter, 1)
    own_scaled = (route_weights[:, :, None] * own_cot[:, None, :].astype(jnp.float32)).astype(
        jnp.bfloat16
    )
    own_scaled = own_scaled.reshape(slot_total, quarter)
    arrived = (
        lax.all_to_all(own_input[source_rows], "sp", split_axis=0, concat_axis=0, tiled=True),
        lax.all_to_all(own_scaled[sorting], "sp", split_axis=0, concat_axis=0, tiled=True),
    )
    routed, routed_cot = (
        lax.all_gather(arrived[0], "tp", axis=1, tiled=True),
        lax.all_gather(arrived[1], "tp", axis=1, tiled=True),
    )
    grad_gate, grad_up, grad_down, partial_value = expert_pass(
        routed, routed_cot, gate_local, up_local, down_local
    )
    summed = lax.psum_scatter(
        partial_value.astype(jnp.bfloat16), "tp", scatter_dimension=1, tiled=True
    )
    returned = lax.all_to_all(summed, "sp", split_axis=0, concat_axis=0, tiled=True)
    per_slot = returned[inverse].reshape(tok_count, 2, quarter).astype(jnp.float32)
    own_grad = (own_cot.astype(jnp.float32) + per_slot[:, 0] + per_slot[:, 1]).astype(jnp.bfloat16)
    token_grad = lax.all_gather(own_grad, "tp", axis=1, tiled=True)
    delta_mixer = jnp.dot(token_grad, out_weight, preferred_element_type=jnp.float32).astype(
        jnp.bfloat16
    )
    grad_out_weight = lax.psum_scatter(
        jnp.dot(token_grad.T, mixer_out, preferred_element_type=jnp.float32),
        "sp",
        scatter_dimension=0,
        tiled=True,
    )
    gradients = mixer_backward(query_vectors, key_vectors, value_vectors, log_decay, delta_mixer)
    return (
        grad_gate[None],
        grad_up[None],
        grad_down[None],
        grad_out_weight,
        gradients[0],
        gradients[1],
        gradients[2],
        gradients[3],
    )


def solution(mesh):
    return jax.shard_map(
        shards,
        mesh=mesh,
        in_specs=(
            P("sp", None),
            P("sp", None),
            P("sp", None),
            P("sp", None),
            P("sp", None, "tp"),
            P("sp", None, "tp"),
            P("sp", "tp", None),
            P(None, "tp"),
            P("sp", "tp"),
            P("sp", "tp"),
            P("sp", "tp"),
            P("sp", "tp"),
            P("sp", "tp"),
        ),
        out_specs=(
            P("sp", None, "tp"),
            P("sp", None, "tp"),
            P("sp", "tp", None),
            P("sp", "tp"),
            P("sp", "tp"),
            P("sp", "tp"),
            P("sp", "tp"),
            P("sp", "tp"),
        ),
        check_vma=False,
    )
```

profile of v0, /device:TPU:0, one launch (start us, length us, event | category | flops | bytes accessed | tf_op | source)
XLA Modules:
  0.0 286.6 jit_solution(11970388747778692487)
XLA Ops:
  8.3 3.8 %sort.34 = (s32[512]{0:T(512)}, s32[512]{0:T(512)S(1)}) sort(s32[512]{0:T(512)S(1)} %reshape.170, s32[512]{0:T(512)S(1)} %iota.42), dimensions={0}, to_apply=%region_0.0 | sort | flops 4608 | bytes 8192 | tf_op jit(solution)/shard_map/jit(argsort)/sort | solution.py:168
  13.2 2.0 gather_fusion
  15.2 21.7 %all_to_all.36 = bf16[8,64,512]{2,1,0:T(8,128)(2,1)} all-to-all(bf16[8,64,512]{2,1,0:T(8,128)(2,1)S(1)} %bitcast.315), channel_id=1, replica_groups=mesh['sp'=8,'tp'=4] {'sp'}, dimensions={0} | all-to-all | bytes 1048576 | tf_op jit(solution)/shard_map/all_to_all | solution.py:183
  38.5 2.0 gather_fusion.1
  40.5 17.8 %all_to_all.37 = bf16[8,64,512]{2,1,0:T(8,128)(2,1)} all-to-all(bf16[8,64,512]{2,1,0:T(8,128)(2,1)S(1)} %bitcast.316), channel_id=1, replica_groups=mesh['sp'=8,'tp'=4] {'sp'}, dimensions={0} | all-to-all | bytes 1048576 | tf_op jit(solution)/shard_map/all_to_all | solution.py:184
  58.7 2.3 fusion.32
  61.0 2.5 fusion.35
  63.5 19.3 %all-gather.9.cloned.1.call-done = bf16[512,2048]{1,0:T(8,128)(2,1)} async-done(((bf16[512,512]{1,0:T(8,128)(2,1)}), bf16[512,2048]{1,0:T(8,128)(2,1)}) %all-gather.9.cloned.1.call-update) | async-done | bytes 2097168 | tf_op jit(solution)/shard_map/all_gather | solution.py:188
  82.8 2.7 multiply_convert_fusion.2
  87.0 2.1 add_convert_fusion
  91.7 20.5 %all-gather.1 = f32[16,1,64]{2,1,0:T(1,128)S(1)} all-gather(f32[2,1,64]{2,1,0:T(1,128)S(1)} %bitcast.346), channel_id=3, replica_groups=mesh['sp'=8,'tp'=4] {'sp'}, dimensions={0}, use_global_device_ids=true | all-gather | bytes 4608 | tf_op jit(solution)/shard_map/all_gather | solution.py:14
  112.9 31.5 %all-gather.2 = f32[16,64,128]{2,1,0:T(8,128)S(1)} all-gather(f32[2,64,128]{2,1,0:T(8,128)S(1)} %fusion.43), channel_id=4, replica_groups=mesh['sp'=8,'tp'=4] {'sp'}, dimensions={0}, use_global_device_ids=true | all-gather | bytes 589824 | tf_op jit(solution)/shard_map/all_gather | solution.py:14
  144.5 3.5 %all-to-all-start.2 = ((bf16[8,64,512]{2,1,0:T(8,128)(2,1)}), bf16[8,64,512]{2,1,0:T(8,128)(2,1)S(1)}, u32[]{:S(2)}, u32[]{:S(2)}) async-start(bf16[8,64,512]{2,1,0:T(8,128)(2,1)} %bitcast.335), calls=%async_computation.3 | async-start | bytes 1048576 | tf_op jit(solution)/shard_map/all_to_all | solution.py:196
  149.5 3.8 %sort.35 = (s32[512]{0:T(512)}, s32[512]{0:T(512)S(1)}) sort(s32[512]{0:T(512)S(1)} %get-tuple-element.514, s32[512]{0:T(512)S(1)} %iota.43), dimensions={0}, to_apply=%region_2.3 | sort | flops 4608 | bytes 8192 | tf_op jit(solution)/shard_map/jit(argsort)/sort | solution.py:170
  153.8 4.4 %all-to-all-done.2 = bf16[8,64,512]{2,1,0:T(8,128)(2,1)S(1)} async-done(((bf16[8,64,512]{2,1,0:T(8,128)(2,1)}), bf16[8,64,512]{2,1,0:T(8,128)(2,1)S(1)}, u32[]{:S(2)}, u32[]{:S(2)}) %all-to-all-start.2) | async-done | bytes 524320 | tf_op jit(solution)/shard_map/all_to_all | solution.py:196
  158.2 2.6 gather_fusion.2
  165.2 5.1 %while.64 = (s32[]{:T(128)}, f32[2,64,128]{2,1,0:T(8,128)S(1)}, f32[4,2,64,128]{3,2,1,0:T(8,128)}, f32[4,2,64,64]{3,2,1,0:T(8,128)S(1)}, f32[4,2,64,64]{2,0,3,1:...) while((s32[]{:T(128)}, f32[2,64,128]{2,1,0:T(8,128)S(1)}, ...), condition=%wide.region_12.13_spmd, body=%wide.region_10.12_spmd.sunk | while | flops 13148162 | bytes 725105 | solution.py:59
  171.2 3.4 %fusion.27 = bf16[1,2048,256]{2,1,0:T(8,128)(2,1)} fusion(bf16[512,2048]{1,0:T(8,128)(2,1)} %all-gather.7.cloned.1.call-done, bf16[512,256]{1,0:T(8,128)(2,1)S(1)} %copy-done.13), kind=kOutput, calls=%fused_computation.70 | convolution fusion | flops 537395200 | bytes 3407872 | tf_op jit(solution)/shard_map/dot_general | solution.py:90
  174.6 2.8 fusion.28
  180.2 3.2 %fusion.57 = f32[2048,256]{1,0:T(8,128)} fusion(bf16[256,2048]{1,0:T(8,128)(2,1)} %all-gather.11.cloned.1.call-done, bf16[256,256]{1,0:T(8,128)(2,1)} %param.29), kind=kOutput, calls=%fused_computation.131 | convolution fusion | flops 268435456 | bytes 3276800 | tf_op jit(solution)/shard_map/dot_general | solution.py:204
  183.4 2.4 convolution_convert_fusion.3
  187.2 32.7 %all-gather = f32[16,64,128]{2,1,0:T(8,128)S(1)} all-gather(f32[2,64,128]{2,1,0:T(8,128)S(1)} %fusion.45), channel_id=2, replica_groups=mesh['sp'=8,'tp'=4] {'sp'}, dimensions={0}, use_global_device_ids=true | all-gather | bytes 589824 | tf_op jit(solution)/shard_map/all_gather | solution.py:14
  221.9 52.6 %while.65 = (s32[]{:T(128)}, f32[2,64,128]{2,1,0:T(8,128)S(1)}, f32[4,2,64,64]{3,1,2,0:T(2,128)S(1)}, bf16[4,2,64,64]{3,1,2,0:T(2,128)(2,1)}, bf16[4,2,64,128]{3...) while((s32[]{:T(128)}, f32[2,64,128]{2,1,0:T(8,128)S(1)}, ...), condition=%wide.region_20.21_spmd, body=%wide.region_13.20_spmd.sunk | while | flops 87216128 | bytes 5496629 | solution.py:59
  224.2 4.1 %fusion.124 = (f32[2,64,64]{2,1,0:T(8,128)S(1)}, f32[2,64,64]{2,1,0:T(8,128)S(1)}, f32[2,64,64]{2,1,0:T(8,128)S(1)}) fusion(f32[2,64,64]{1,2,0:T(8,128)S(1)} %copy.335, f32[2,64,64]{1,2,0:T(8,128)S(1)} %copy.336, f32[2,64,64]{2,1,0:T(8,128)S(1)} %reduce_window_sum.59, f32[2,64,64]{2,1,0:T(8,128)S(1)} %fusion.123, ...), kind=kLoop, calls=%fused_computation.32.clone.1 | loop fusion | flops 5218304 | bytes 233472 | tf_op jit(solution)/shard_map/transpose(jvp())/while/body/eval_jaxpr/checkpoint/reduce_sum | solution.py:38
  229.2 2.0 fusion.131
  231.1 2.0 fusion.132
  237.3 4.1 %fusion.124 = (f32[2,64,64]{2,1,0:T(8,128)S(1)}, f32[2,64,64]{2,1,0:T(8,128)S(1)}, f32[2,64,64]{2,1,0:T(8,128)S(1)}) fusion(f32[2,64,64]{1,2,0:T(8,128)S(1)} %copy.335, f32[2,64,64]{1,2,0:T(8,128)S(1)} %copy.336, f32[2,64,64]{2,1,0:T(8,128)S(1)} %reduce_window_sum.59, f32[2,64,64]{2,1,0:T(8,128)S(1)} %fusion.123, ...), kind=kLoop, calls=%fused_computation.32.clone.1 | loop fusion | flops 5218304 | bytes 233472 | tf_op jit(solution)/shard_map/transpose(jvp())/while/body/eval_jaxpr/checkpoint/reduce_sum | solution.py:38
  244.3 2.0 fusion.132
  250.5 4.1 %fusion.124 = (f32[2,64,64]{2,1,0:T(8,128)S(1)}, f32[2,64,64]{2,1,0:T(8,128)S(1)}, f32[2,64,64]{2,1,0:T(8,128)S(1)}) fusion(f32[2,64,64]{1,2,0:T(8,128)S(1)} %copy.335, f32[2,64,64]{1,2,0:T(8,128)S(1)} %copy.336, f32[2,64,64]{2,1,0:T(8,128)S(1)} %reduce_window_sum.59, f32[2,64,64]{2,1,0:T(8,128)S(1)} %fusion.123, ...), kind=kLoop, calls=%fused_computation.32.clone.1 | loop fusion | flops 5218304 | bytes 233472 | tf_op jit(solution)/shard_map/transpose(jvp())/while/body/eval_jaxpr/checkpoint/reduce_sum | solution.py:38
  257.4 2.0 fusion.132
  263.7 4.1 %fusion.124 = (f32[2,64,64]{2,1,0:T(8,128)S(1)}, f32[2,64,64]{2,1,0:T(8,128)S(1)}, f32[2,64,64]{2,1,0:T(8,128)S(1)}) fusion(f32[2,64,64]{1,2,0:T(8,128)S(1)} %copy.335, f32[2,64,64]{1,2,0:T(8,128)S(1)} %copy.336, f32[2,64,64]{2,1,0:T(8,128)S(1)} %reduce_window_sum.59, f32[2,64,64]{2,1,0:T(8,128)S(1)} %fusion.123, ...), kind=kLoop, calls=%fused_computation.32.clone.1 | loop fusion | flops 5218304 | bytes 233472 | tf_op jit(solution)/shard_map/transpose(jvp())/while/body/eval_jaxpr/checkpoint/reduce_sum | solution.py:38
  270.6 2.0 fusion.132
  (319 shorter events, 59.7 us)
Async XLA Ops:
  7.2 51.5 %copy-start = (bf16[1,2048,256]{2,1,0:T(8,128)(2,1)S(1)}, bf16[1,2048,256]{2,1,0:T(8,128)(2,1)}, u32[]{:S(2)}) copy-start(bf16[1,2048,256]{2,1,0:T(8,128)(2,1)} %param.25) | copy-start | bytes 3145732
  7.2 51.5 %all-gather.7.cloned.1.call-start = ((), (), s32[]{:S(2)}) async-start(), calls=%async_computation.5 | async-start | bytes 2621440 | tf_op jit(solution)/shard_map/all_gather | solution.py:187
  13.2 24.9 %copy-start.19 = (f32[256,2]{0,1:T(2,128)S(1)}, f32[256,2]{0,1:T(2,128)}, u32[]{:S(2)}) copy-start(f32[256,2]{0,1:T(2,128)} %param.24) | copy-start | bytes 6148
  36.9 45.9 %all-gather.9.cloned.1.call-start = ((), (), s32[]{:S(2)}) async-start(), calls=%async_computation.6 | async-start | bytes 2621440 | tf_op jit(solution)/shard_map/all_gather | solution.py:188
  40.5 20.5 %copy-start.3 = (bf16[1,2048,256]{2,1,0:T(8,128)(2,1)S(1)}, bf16[1,2048,256]{2,1,0:T(8,128)(2,1)}, u32[]{:S(2)}) copy-start(bf16[1,2048,256]{2,1,0:T(8,128)(2,1)} %param.26) | copy-start | bytes 3145732
  58.3 86.2 %reduce-scatter.3.cloned.1.call-start = ((), (), s32[]{:S(2)}) async-start(), calls=%async_computation.7 | async-start | bytes 2621440 | tf_op jit(solution)/shard_map/reduce_scatter | solution.py:193
  61.0 24.5 %copy-start.8 = (f32[512,256]{1,0:T(8,128)}, f32[512,256]{1,0:T(8,128)S(1)}, u32[]{:S(2)}) copy-start(f32[512,256]{1,0:T(8,128)S(1)} %fusion.32) | copy-start | bytes 1572868
  63.5 23.5 %copy-start.10 = (f32[512,256]{1,0:T(8,128)}, f32[512,256]{1,0:T(8,128)S(1)}, u32[]{:S(2)}) copy-start(f32[512,256]{1,0:T(8,128)S(1)} %fusion.35) | copy-start | bytes 1572868
  85.5 0.7 copy-start.12
  85.5 1.5 copy-start.14
  87.0 2.2 copy-start.17
  87.0 2.4 copy-start.15
  87.0 4.2 %copy-start.18 = (bf16[256,128]{1,0:T(8,128)(2,1)S(1)}, bf16[256,128]{1,0:T(8,128)(2,1)}, u32[]{:S(2)}) copy-start(bf16[256,128]{1,0:T(8,128)(2,1)} %param.30) | copy-start | bytes 196612
  89.1 2.4 copy-start.16
  144.5 13.7 %all-to-all-start.2 = ((bf16[8,64,512]{2,1,0:T(8,128)(2,1)}), bf16[8,64,512]{2,1,0:T(8,128)(2,1)S(1)}, u32[]{:S(2)}, u32[]{:S(2)}) async-start(bf16[8,64,512]{2,1,0:T(8,128)(2,1)} %bitcast.335), calls=%async_computation.3 | async-start | bytes 1048576 | tf_op jit(solution)/shard_map/all_to_all | solution.py:196
  148.0 32.3 %all-gather.11.cloned.1.call-start = ((), (), s32[]{:S(2)}) async-start(), calls=%async_computation.8 | async-start | bytes 1310720 | tf_op jit(solution)/shard_map/all_gather | solution.py:199
  163.3 7.9 %copy-start.13 = (bf16[512,256]{1,0:T(8,128)(2,1)S(1)}, bf16[512,256]{1,0:T(8,128)(2,1)}, u32[]{:S(2)}) copy-start(bf16[512,256]{1,0:T(8,128)(2,1)} %copy-done.12) | copy-start | bytes 786436
  165.2 114.9 %reduce-scatter.5.cloned.1.call-start = ((), (), s32[]{:S(2)}) async-start(), calls=%async_computation.9 | async-start | bytes 2359296 | tf_op jit(solution)/shard_map/reduce_scatter | solution.py:203
  170.5 4.1 %copy-start.20 = (bf16[512,2048]{1,0:T(8,128)(2,1)S(1)}, bf16[512,2048]{1,0:T(8,128)(2,1)}, u32[]{:S(2)}) copy-start(bf16[512,2048]{1,0:T(8,128)(2,1)} %all-gather.7.cloned.1.call-done) | copy-start | bytes 6291460
  174.6 2.9 copy-start.2
  174.6 2.9 copy-start.9
  174.6 2.9 copy-start.11
  180.2 3.2 %copy-start.1 = (bf16[256,2048]{1,0:T(8,128)(2,1)S(1)}, bf16[256,2048]{1,0:T(8,128)(2,1)}, u32[]{:S(2)}) copy-start(bf16[256,2048]{1,0:T(8,128)(2,1)} %all-gather.11.cloned.1.call-done) | copy-start | bytes 3145732
  223.2 9.9 %copy-start.4 = (bf16[4,2,64,64]{3,1,2,0:T(2,128)(2,1)S(1)}, bf16[4,2,64,64]{3,1,2,0:T(2,128)(2,1)}, u32[]{:S(2)}) copy-start(bf16[4,2,64,64]{3,1,2,0:T(2,128)(2,1)} %get-tuple-element.1077) | copy-start | bytes 196612 | tf_op jit(solution)/shard_map/transpose(jvp())/while
  223.2 10.2 %copy-start.6 = (bf16[4,2,64,128]{3,2,0,1:T(8,128)(2,1)S(1)}, bf16[4,2,64,128]{3,2,0,1:T(8,128)(2,1)}, u32[]{:S(2)}) copy-start(bf16[4,2,64,128]{3,2,0,1:T(8,128)(2,1)} %get-tuple-element.1078) | copy-start | bytes 393220 | tf_op jit(solution)/shard_map/transpose(jvp())/while
  233.8 0.7 copy-start.7
  236.4 9.9 %copy-start.4 = (bf16[4,2,64,64]{3,1,2,0:T(2,128)(2,1)S(1)}, bf16[4,2,64,64]{3,1,2,0:T(2,128)(2,1)}, u32[]{:S(2)}) copy-start(bf16[4,2,64,64]{3,1,2,0:T(2,128)(2,1)} %get-tuple-element.1077) | copy-start | bytes 196612 | tf_op jit(solution)/shard_map/transpose(jvp())/while
  236.4 10.2 %copy-start.6 = (bf16[4,2,64,128]{3,2,0,1:T(8,128)(2,1)S(1)}, bf16[4,2,64,128]{3,2,0,1:T(8,128)(2,1)}, u32[]{:S(2)}) copy-start(bf16[4,2,64,128]{3,2,0,1:T(8,128)(2,1)} %get-tuple-element.1078) | copy-start | bytes 393220 | tf_op jit(solution)/shard_map/transpose(jvp())/while
  249.5 9.9 %copy-start.4 = (bf16[4,2,64,64]{3,1,2,0:T(2,128)(2,1)S(1)}, bf16[4,2,64,64]{3,1,2,0:T(2,128)(2,1)}, u32[]{:S(2)}) copy-start(bf16[4,2,64,64]{3,1,2,0:T(2,128)(2,1)} %get-tuple-element.1077) | copy-start | bytes 196612 | tf_op jit(solution)/shard_map/transpose(jvp())/while
  249.6 10.2 %copy-start.6 = (bf16[4,2,64,128]{3,2,0,1:T(8,128)(2,1)S(1)}, bf16[4,2,64,128]{3,2,0,1:T(8,128)(2,1)}, u32[]{:S(2)}) copy-start(bf16[4,2,64,128]{3,2,0,1:T(8,128)(2,1)} %get-tuple-element.1078) | copy-start | bytes 393220 | tf_op jit(solution)/shard_map/transpose(jvp())/while
  262.7 9.9 %copy-start.4 = (bf16[4,2,64,64]{3,1,2,0:T(2,128)(2,1)S(1)}, bf16[4,2,64,64]{3,1,2,0:T(2,128)(2,1)}, u32[]{:S(2)}) copy-start(bf16[4,2,64,64]{3,1,2,0:T(2,128)(2,1)} %get-tuple-element.1077) | copy-start | bytes 196612 | tf_op jit(solution)/shard_map/transpose(jvp())/while
  262.7 10.2 %copy-start.6 = (bf16[4,2,64,128]{3,2,0,1:T(8,128)(2,1)S(1)}, bf16[4,2,64,128]{3,2,0,1:T(8,128)(2,1)}, u32[]{:S(2)}) copy-start(bf16[4,2,64,128]{3,2,0,1:T(8,128)(2,1)} %get-tuple-element.1078) | copy-start | bytes 393220 | tf_op jit(solution)/shard_map/transpose(jvp())/while
  (7 other events, 4.6 us)
Sparse Core Ops, SparseCore 0:
  37.0 21.5 all-gather.6
  60.2 22.5 all-gather.8
  89.3 31.1 reduce-scatter.2
  165.3 14.8 all-gather.10
  184.2 70.5 reduce-scatter.4
where the time goes:
time: 287 us
  blocking collectives  124 us (43%)
  other arithmetic  53.2 us (19%)
  local copies, waits for them, and re-layouts  32.3 us (11%)
  matrix products  31.7 us (11%)
  waiting for transfers between devices  25.1 us (9%)
  between operations  14.4 us (5%)
  starting transfers between devices  3.88 us (1%)
    all_gather x3, blocking collectives, entering(): everything = jax.tree.map(lambda part: lax.all_gather(part, axis), shard)  84.7 us
    all_to_all x1, blocking collectives, shards(): lax.all_to_all(own_input[source_rows], 'sp', split_axis=0, concat_axis=0,...  21.7 us
    all_gather x1, waiting for transfers between devices, shards(): lax.all_gather(arrived[1], 'tp', axis=1, tiled=True)  19.3 us
    all_to_all x1, blocking collectives, shards(): lax.all_to_all(own_scaled[sorting], 'sp', split_axis=0, concat_axis=0, ti...  17.8 us
    reduce_sum x4, other arithmetic, block_step(): difference = cumulative[:, :, None, :] - cumulative[:, None, :, :]  16.3 us
    while x8, other arithmetic  16 us
  transfers between devices with their start and end apart: 6, of which 4 were waited for; matrix products, arithmetic and copies ran while one was open for 32% of the time, Pallas kernels for 0%

commit v1 on v0

--- a/solution.py
+++ b/solution.py
@@ -185,7 +185,7 @@
     )
     routed, routed_cot = (
         lax.all_gather(arrived[0], "tp", axis=1, tiled=True),
-        lax.all_gather(arrived[1], "tp", axis=1, tiled=True),
+        jnp.concatenate(jax.lax.all_gather(arrived[1], "tp"), axis=1),
     )
     grad_gate, grad_up, grad_down, partial_value = expert_pass(
         routed, routed_cot, gate_local, up_local, down_local

time: 287 us -> 290 us (1.010)
  local copies, waits for them, and re-layouts: 32.3 us -> 35.5 us
  transfers between devices with their start and end apart: 6 -> 6, of which waited for: 4 -> 4; matrix products, arithmetic and copies ran while one was open for 32% -> 31% of each run, Pallas kernels for 0% -> 0%
where the time goes in v1:
time: 290 us
  blocking collectives  124 us (43%)
  other arithmetic  53.2 us (18%)
  local copies, waits for them, and re-layouts  35.5 us (12%)
  matrix products  32.4 us (11%)
  waiting for transfers between devices  24.4 us (8%)
  between operations  14.3 us (5%)
  starting transfers between devices  3.88 us (1%)
    all_gather x3, blocking collectives, entering(): everything = jax.tree.map(lambda part: lax.all_gather(part, axis), shard)  84.5 us
    all_to_all x1, blocking collectives, shards(): lax.all_to_all(own_input[source_rows], 'sp', split_axis=0, concat_axis=0,...  21.7 us
    all_gather x1, waiting for transfers between devices, shards(): jax.lax.all_gather(arrived[1], 'tp')  17.9 us
    all_to_all x1, blocking collectives, shards(): lax.all_to_all(own_scaled[sorting], 'sp', split_axis=0, concat_axis=0, ti...  17.8 us
    reduce_sum x4, other arithmetic, block_step(): difference = cumulative[:, :, None, :] - cumulative[:, None, :, :]  16.3 us
    while x8, other arithmetic  16 us
  transfers between devices with their start and end apart: 6, of which 4 were waited for; matrix products, arithmetic and copies ran while one was open for 31% of the time, Pallas kernels for 0%

profile of v1, /device:TPU:0, one launch (start us, length us, event | category | flops | bytes accessed | tf_op | source)
XLA Modules:
  0.0 289.6 jit_solution(11537079997160557225)
XLA Ops:
  8.3 3.8 %sort.34 = (s32[512]{0:T(512)}, s32[512]{0:T(512)S(1)}) sort(s32[512]{0:T(512)S(1)} %reshape.177, s32[512]{0:T(512)S(1)} %iota.42), dimensions={0}, to_apply=%region_0.0 | sort | flops 4608 | bytes 8192 | tf_op jit(solution)/shard_map/jit(argsort)/sort | solution.py:168
  13.2 2.0 gather_fusion
  15.2 21.7 %all_to_all.33 = bf16[8,64,512]{2,1,0:T(8,128)(2,1)} all-to-all(bf16[8,64,512]{2,1,0:T(8,128)(2,1)S(1)} %bitcast.318), channel_id=1, replica_groups=mesh['sp'=8,'tp'=4] {'sp'}, dimensions={0} | all-to-all | bytes 1048576 | tf_op jit(solution)/shard_map/all_to_all | solution.py:183
  38.5 2.0 gather_fusion.1
  40.5 17.8 %all_to_all.34 = bf16[8,64,512]{2,1,0:T(8,128)(2,1)} all-to-all(bf16[8,64,512]{2,1,0:T(8,128)(2,1)S(1)} %bitcast.319), channel_id=1, replica_groups=mesh['sp'=8,'tp'=4] {'sp'}, dimensions={0} | all-to-all | bytes 1048576 | tf_op jit(solution)/shard_map/all_to_all | solution.py:184
  58.7 3.1 %fusion.32 = f32[512,256]{1,0:T(8,128)} fusion(bf16[512,2048]{1,0:T(8,128)(2,1)} %all-gather.7.cloned.1.call-done, bf16[1,2048,256]{2,1,0:T(8,128)(2,1)S(1)} %copy-done), kind=kOutput, calls=%fused_computation.76 | convolution fusion | flops 536870912 | bytes 3670016 | tf_op jit(solution)/shard_map/dot_general | solution.py:77
  61.8 3.1 %fusion.35 = f32[512,256]{1,0:T(8,128)} fusion(bf16[512,2048]{1,0:T(8,128)(2,1)} %all-gather.7.cloned.1.call-done, bf16[1,2048,256]{2,1,0:T(8,128)(2,1)S(1)} %copy-done.4), kind=kOutput, calls=%fused_computation.79 | convolution fusion | flops 536870912 | bytes 3670016 | tf_op jit(solution)/shard_map/dot_general | solution.py:78
  64.9 17.9 %all-gather.9.cloned.1.call-done = bf16[4,512,512]{2,1,0:T(8,128)(2,1)} async-done(((bf16[1,512,512]{2,1,0:T(8,128)(2,1)}), bf16[4,512,512]{2,1,0:T(8,128)(2,1)}) %all-gather.9.cloned.1.call-update) | async-done | bytes 2097168 | tf_op jit(solution)/shard_map/all_gather | solution.py:188
  82.8 2.8 copy.185
  85.6 3.1 %multiply_convert_fusion.2 = (bf16[512,256]{1,0:T(8,128)(2,1)S(1)}, bf16[512,256]{1,0:T(8,128)(2,1)S(1)}) fusion(f32[512,256]{1,0:T(8,128)} %fusion.32, f32[512,256]{1,0:T(8,128)} %fusion.35, bf16[512,2048]{0,1:T(8,128)(2,1)S(1)} %bitcast.320, bf16[1,256,2048]{2,1,0:T(8,128)(2,1)} %param.27), kind=kOutput, calls=%fused_computation.90 | convolution fusion | flops 538574848 | bytes 4718592 | tf_op jit(solution)/shard_map/dot_general | solution.py:82
  90.2 2.1 add_convert_fusion
  94.8 20.5 %all-gather.1 = f32[16,1,64]{2,1,0:T(1,128)S(1)} all-gather(f32[2,1,64]{2,1,0:T(1,128)S(1)} %bitcast.351), channel_id=3, replica_groups=mesh['sp'=8,'tp'=4] {'sp'}, dimensions={0}, use_global_device_ids=true | all-gather | bytes 4608 | tf_op jit(solution)/shard_map/all_gather | solution.py:14
  116.1 31.6 %all-gather.2 = f32[16,64,128]{2,1,0:T(8,128)S(1)} all-gather(f32[2,64,128]{2,1,0:T(8,128)S(1)} %fusion.43), channel_id=4, replica_groups=mesh['sp'=8,'tp'=4] {'sp'}, dimensions={0}, use_global_device_ids=true | all-gather | bytes 589824 | tf_op jit(solution)/shard_map/all_gather | solution.py:14
  147.6 3.5 %all-to-all-start.2 = ((bf16[8,64,512]{2,1,0:T(8,128)(2,1)}), bf16[8,64,512]{2,1,0:T(8,128)(2,1)S(1)}, u32[]{:S(2)}, u32[]{:S(2)}) async-start(bf16[8,64,512]{2,1,0:T(8,128)(2,1)} %bitcast.340), calls=%async_computation.3 | async-start | bytes 1048576 | tf_op jit(solution)/shard_map/all_to_all | solution.py:196
  152.6 3.8 %sort.35 = (s32[512]{0:T(512)}, s32[512]{0:T(512)S(1)}) sort(s32[512]{0:T(512)S(1)} %get-tuple-element.514, s32[512]{0:T(512)S(1)} %iota.43), dimensions={0}, to_apply=%region_2.3 | sort | flops 4608 | bytes 8192 | tf_op jit(solution)/shard_map/jit(argsort)/sort | solution.py:170
  156.9 4.4 %all-to-all-done.2 = bf16[8,64,512]{2,1,0:T(8,128)(2,1)S(1)} async-done(((bf16[8,64,512]{2,1,0:T(8,128)(2,1)}), bf16[8,64,512]{2,1,0:T(8,128)(2,1)S(1)}, u32[]{:S(2)}, u32[]{:S(2)}) %all-to-all-start.2) | async-done | bytes 524320 | tf_op jit(solution)/shard_map/all_to_all | solution.py:196
  161.3 2.6 gather_fusion.2
  168.4 5.1 %while.64 = (s32[]{:T(128)}, f32[2,64,128]{2,1,0:T(8,128)S(1)}, f32[4,2,64,128]{3,2,1,0:T(8,128)}, f32[4,2,64,64]{3,2,1,0:T(8,128)S(1)}, f32[4,2,64,64]{2,0,3,1:...) while((s32[]{:T(128)}, f32[2,64,128]{2,1,0:T(8,128)S(1)}, ...), condition=%wide.region_12.13_spmd, body=%wide.region_10.12_spmd.sunk | while | flops 13148162 | bytes 725105 | solution.py:59
  174.4 3.4 %fusion.27 = bf16[1,2048,256]{2,1,0:T(8,128)(2,1)} fusion(bf16[512,2048]{1,0:T(8,128)(2,1)} %all-gather.7.cloned.1.call-done, bf16[512,256]{1,0:T(8,128)(2,1)S(1)} %copy-done.11), kind=kOutput, calls=%fused_computation.70 | convolution fusion | flops 537395200 | bytes 3407872 | tf_op jit(solution)/shard_map/dot_general | solution.py:90
  183.4 3.2 %fusion.57 = f32[2048,256]{1,0:T(8,128)} fusion(bf16[256,2048]{1,0:T(8,128)(2,1)} %all-gather.11.cloned.1.call-done, bf16[256,256]{1,0:T(8,128)(2,1)} %param.29), kind=kOutput, calls=%fused_computation.131 | convolution fusion | flops 268435456 | bytes 3276800 | tf_op jit(solution)/shard_map/dot_general | solution.py:204
  186.6 2.4 convolution_convert_fusion.3
  190.4 32.5 %all-gather = f32[16,64,128]{2,1,0:T(8,128)S(1)} all-gather(f32[2,64,128]{2,1,0:T(8,128)S(1)} %fusion.45), channel_id=2, replica_groups=mesh['sp'=8,'tp'=4] {'sp'}, dimensions={0}, use_global_device_ids=true | all-gather | bytes 589824 | tf_op jit(solution)/shard_map/all_gather | solution.py:14
  224.8 52.6 %while.65 = (s32[]{:T(128)}, f32[2,64,128]{2,1,0:T(8,128)S(1)}, f32[4,2,64,64]{3,1,2,0:T(2,128)S(1)}, bf16[4,2,64,64]{3,1,2,0:T(2,128)(2,1)}, bf16[4,2,64,128]{3...) while((s32[]{:T(128)}, f32[2,64,128]{2,1,0:T(8,128)S(1)}, ...), condition=%wide.region_20.21_spmd, body=%wide.region_13.20_spmd.sunk | while | flops 87216128 | bytes 5496629 | solution.py:59
  227.1 4.1 %fusion.124 = (f32[2,64,64]{2,1,0:T(8,128)S(1)}, f32[2,64,64]{2,1,0:T(8,128)S(1)}, f32[2,64,64]{2,1,0:T(8,128)S(1)}) fusion(f32[2,64,64]{1,2,0:T(8,128)S(1)} %copy.340, f32[2,64,64]{1,2,0:T(8,128)S(1)} %copy.341, f32[2,64,64]{2,1,0:T(8,128)S(1)} %reduce_window_sum.59, f32[2,64,64]{2,1,0:T(8,128)S(1)} %fusion.123, ...), kind=kLoop, calls=%fused_computation.32.clone.1 | loop fusion | flops 5218304 | bytes 233472 | tf_op jit(solution)/shard_map/transpose(jvp())/while/body/eval_jaxpr/checkpoint/reduce_sum | solution.py:38
  232.1 2.0 fusion.131
  234.1 2.0 fusion.132
  240.3 4.1 %fusion.124 = (f32[2,64,64]{2,1,0:T(8,128)S(1)}, f32[2,64,64]{2,1,0:T(8,128)S(1)}, f32[2,64,64]{2,1,0:T(8,128)S(1)}) fusion(f32[2,64,64]{1,2,0:T(8,128)S(1)} %copy.340, f32[2,64,64]{1,2,0:T(8,128)S(1)} %copy.341, f32[2,64,64]{2,1,0:T(8,128)S(1)} %reduce_window_sum.59, f32[2,64,64]{2,1,0:T(8,128)S(1)} %fusion.123, ...), kind=kLoop, calls=%fused_computation.32.clone.1 | loop fusion | flops 5218304 | bytes 233472 | tf_op jit(solution)/shard_map/transpose(jvp())/while/body/eval_jaxpr/checkpoint/reduce_sum | solution.py:38
  247.2 2.0 fusion.132
  253.4 4.1 %fusion.124 = (f32[2,64,64]{2,1,0:T(8,128)S(1)}, f32[2,64,64]{2,1,0:T(8,128)S(1)}, f32[2,64,64]{2,1,0:T(8,128)S(1)}) fusion(f32[2,64,64]{1,2,0:T(8,128)S(1)} %copy.340, f32[2,64,64]{1,2,0:T(8,128)S(1)} %copy.341, f32[2,64,64]{2,1,0:T(8,128)S(1)} %reduce_window_sum.59, f32[2,64,64]{2,1,0:T(8,128)S(1)} %fusion.123, ...), kind=kLoop, calls=%fused_computation.32.clone.1 | loop fusion | flops 5218304 | bytes 233472 | tf_op jit(solution)/shard_map/transpose(jvp())/while/body/eval_jaxpr/checkpoint/reduce_sum | solution.py:38
  260.4 2.0 fusion.132
  266.6 4.1 %fusion.124 = (f32[2,64,64]{2,1,0:T(8,128)S(1)}, f32[2,64,64]{2,1,0:T(8,128)S(1)}, f32[2,64,64]{2,1,0:T(8,128)S(1)}) fusion(f32[2,64,64]{1,2,0:T(8,128)S(1)} %copy.340, f32[2,64,64]{1,2,0:T(8,128)S(1)} %copy.341, f32[2,64,64]{2,1,0:T(8,128)S(1)} %reduce_window_sum.59, f32[2,64,64]{2,1,0:T(8,128)S(1)} %fusion.123, ...), kind=kLoop, calls=%fused_computation.32.clone.1 | loop fusion | flops 5218304 | bytes 233472 | tf_op jit(solution)/shard_map/transpose(jvp())/while/body/eval_jaxpr/checkpoint/reduce_sum | solution.py:38
  273.5 2.0 fusion.132
  (322 shorter events, 62.4 us)
Async XLA Ops:
  7.2 51.5 %copy-start = (bf16[1,2048,256]{2,1,0:T(8,128)(2,1)S(1)}, bf16[1,2048,256]{2,1,0:T(8,128)(2,1)}, u32[]{:S(2)}) copy-start(bf16[1,2048,256]{2,1,0:T(8,128)(2,1)} %param.25) | copy-start | bytes 3145732
  7.2 51.5 %all-gather.7.cloned.1.call-start = ((), (), s32[]{:S(2)}) async-start(), calls=%async_computation.5 | async-start | bytes 2621440 | tf_op jit(solution)/shard_map/all_gather | solution.py:187
  13.2 24.9 %copy-start.18 = (f32[256,2]{0,1:T(2,128)S(1)}, f32[256,2]{0,1:T(2,128)}, u32[]{:S(2)}) copy-start(f32[256,2]{0,1:T(2,128)} %param.24) | copy-start | bytes 6148
  36.9 45.9 %all-gather.9.cloned.1.call-start = ((), (), s32[]{:S(2)}) async-start(), calls=%async_computation.6 | async-start | bytes 2621440 | tf_op jit(solution)/shard_map/all_gather | solution.py:188
  40.5 21.3 %copy-start.4 = (bf16[1,2048,256]{2,1,0:T(8,128)(2,1)S(1)}, bf16[1,2048,256]{2,1,0:T(8,128)(2,1)}, u32[]{:S(2)}) copy-start(bf16[1,2048,256]{2,1,0:T(8,128)(2,1)} %param.26) | copy-start | bytes 3145732
  58.3 89.3 %reduce-scatter.3.cloned.1.call-start = ((), (), s32[]{:S(2)}) async-start(), calls=%async_computation.7 | async-start | bytes 2621440 | tf_op jit(solution)/shard_map/reduce_scatter | solution.py:193
  85.6 3.9 %copy-start.2 = (bf16[4,512,512]{1,2,0:T(8,128)(2,1)}, bf16[4,512,512]{1,2,0:T(8,128)(2,1)S(1)}, u32[]{:S(2)}) copy-start(bf16[4,512,512]{1,2,0:T(8,128)(2,1)S(1)} %copy.185) | copy-start | bytes 6291460
  88.7 0.8 copy-start.12
  88.7 3.5 %copy-start.10 = (bf16[512,256]{1,0:T(8,128)(2,1)}, bf16[512,256]{1,0:T(8,128)(2,1)S(1)}, u32[]{:S(2)}) copy-start(bf16[512,256]{1,0:T(8,128)(2,1)S(1)} %get-tuple-element.762) | copy-start | bytes 786436
  88.7 1.4 copy-start.5
  90.1 2.1 copy-start.16
  90.1 2.4 copy-start.14
  90.1 4.2 %copy-start.17 = (bf16[256,128]{1,0:T(8,128)(2,1)S(1)}, bf16[256,128]{1,0:T(8,128)(2,1)}, u32[]{:S(2)}) copy-start(bf16[256,128]{1,0:T(8,128)(2,1)} %param.30) | copy-start | bytes 196612
  92.2 2.4 copy-start.15
  147.6 13.7 %all-to-all-start.2 = ((bf16[8,64,512]{2,1,0:T(8,128)(2,1)}), bf16[8,64,512]{2,1,0:T(8,128)(2,1)S(1)}, u32[]{:S(2)}, u32[]{:S(2)}) async-start(bf16[8,64,512]{2,1,0:T(8,128)(2,1)} %bitcast.340), calls=%async_computation.3 | async-start | bytes 1048576 | tf_op jit(solution)/shard_map/all_to_all | solution.py:196
  151.1 32.2 %all-gather.11.cloned.1.call-start = ((), (), s32[]{:S(2)}) async-start(), calls=%async_computation.8 | async-start | bytes 1310720 | tf_op jit(solution)/shard_map/all_gather | solution.py:199
  166.5 7.9 %copy-start.11 = (bf16[512,256]{1,0:T(8,128)(2,1)S(1)}, bf16[512,256]{1,0:T(8,128)(2,1)}, u32[]{:S(2)}) copy-start(bf16[512,256]{1,0:T(8,128)(2,1)} %copy-done.10) | copy-start | bytes 786436
  168.4 114.7 %reduce-scatter.5.cloned.1.call-start = ((), (), s32[]{:S(2)}) async-start(), calls=%async_computation.9 | async-start | bytes 2359296 | tf_op jit(solution)/shard_map/reduce_scatter | solution.py:203
  173.5 4.3 %copy-start.13 = (bf16[512,256]{1,0:T(8,128)(2,1)S(1)}, bf16[512,256]{1,0:T(8,128)(2,1)}, u32[]{:S(2)}) copy-start(bf16[512,256]{1,0:T(8,128)(2,1)} %copy-done.12) | copy-start | bytes 786436
  173.7 4.1 %copy-start.19 = (bf16[512,2048]{1,0:T(8,128)(2,1)S(1)}, bf16[512,2048]{1,0:T(8,128)(2,1)}, u32[]{:S(2)}) copy-start(bf16[512,2048]{1,0:T(8,128)(2,1)} %all-gather.7.cloned.1.call-done) | copy-start | bytes 6291460
  177.7 1.8 copy-start.3
  177.8 1.8 copy-start.20
  177.8 2.2 copy-start.21
  183.4 3.2 %copy-start.1 = (bf16[256,2048]{1,0:T(8,128)(2,1)S(1)}, bf16[256,2048]{1,0:T(8,128)(2,1)}, u32[]{:S(2)}) copy-start(bf16[256,2048]{1,0:T(8,128)(2,1)} %all-gather.11.cloned.1.call-done) | copy-start | bytes 3145732
  226.2 9.9 %copy-start.6 = (bf16[4,2,64,64]{3,1,2,0:T(2,128)(2,1)S(1)}, bf16[4,2,64,64]{3,1,2,0:T(2,128)(2,1)}, u32[]{:S(2)}) copy-start(bf16[4,2,64,64]{3,1,2,0:T(2,128)(2,1)} %get-tuple-element.1077) | copy-start | bytes 196612 | tf_op jit(solution)/shard_map/transpose(jvp())/while
  226.2 10.2 %copy-start.8 = (bf16[4,2,64,128]{3,2,0,1:T(8,128)(2,1)S(1)}, bf16[4,2,64,128]{3,2,0,1:T(8,128)(2,1)}, u32[]{:S(2)}) copy-start(bf16[4,2,64,128]{3,2,0,1:T(8,128)(2,1)} %get-tuple-element.1078) | copy-start | bytes 393220 | tf_op jit(solution)/shard_map/transpose(jvp())/while
  239.3 9.9 %copy-start.6 = (bf16[4,2,64,64]{3,1,2,0:T(2,128)(2,1)S(1)}, bf16[4,2,64,64]{3,1,2,0:T(2,128)(2,1)}, u32[]{:S(2)}) copy-start(bf16[4,2,64,64]{3,1,2,0:T(2,128)(2,1)} %get-tuple-element.1077) | copy-start | bytes 196612 | tf_op jit(solution)/shard_map/transpose(jvp())/while
  239.3 10.2 %copy-start.8 = (bf16[4,2,64,128]{3,2,0,1:T(8,128)(2,1)S(1)}, bf16[4,2,64,128]{3,2,0,1:T(8,128)(2,1)}, u32[]{:S(2)}) copy-start(bf16[4,2,64,128]{3,2,0,1:T(8,128)(2,1)} %get-tuple-element.1078) | copy-start | bytes 393220 | tf_op jit(solution)/shard_map/transpose(jvp())/while
  252.5 9.9 %copy-start.6 = (bf16[4,2,64,64]{3,1,2,0:T(2,128)(2,1)S(1)}, bf16[4,2,64,64]{3,1,2,0:T(2,128)(2,1)}, u32[]{:S(2)}) copy-start(bf16[4,2,64,64]{3,1,2,0:T(2,128)(2,1)} %get-tuple-element.1077) | copy-start | bytes 196612 | tf_op jit(solution)/shard_map/transpose(jvp())/while
  252.5 10.2 %copy-start.8 = (bf16[4,2,64,128]{3,2,0,1:T(8,128)(2,1)S(1)}, bf16[4,2,64,128]{3,2,0,1:T(8,128)(2,1)}, u32[]{:S(2)}) copy-start(bf16[4,2,64,128]{3,2,0,1:T(8,128)(2,1)} %get-tuple-element.1078) | copy-start | bytes 393220 | tf_op jit(solution)/shard_map/transpose(jvp())/while
  265.6 9.9 %copy-start.6 = (bf16[4,2,64,64]{3,1,2,0:T(2,128)(2,1)S(1)}, bf16[4,2,64,64]{3,1,2,0:T(2,128)(2,1)}, u32[]{:S(2)}) copy-start(bf16[4,2,64,64]{3,1,2,0:T(2,128)(2,1)} %get-tuple-element.1077) | copy-start | bytes 196612 | tf_op jit(solution)/shard_map/transpose(jvp())/while
  265.6 10.2 %copy-start.8 = (bf16[4,2,64,128]{3,2,0,1:T(8,128)(2,1)S(1)}, bf16[4,2,64,128]{3,2,0,1:T(8,128)(2,1)}, u32[]{:S(2)}) copy-start(bf16[4,2,64,128]{3,2,0,1:T(8,128)(2,1)} %get-tuple-element.1078) | copy-start | bytes 393220 | tf_op jit(solution)/shard_map/transpose(jvp())/while
  (8 other events, 5.3 us)
Sparse Core Ops, SparseCore 0:
  37.0 21.5 all-gather.6
  60.2 22.5 all-gather.8
  92.4 31.1 reduce-scatter.2
  168.5 14.8 all-gather.10
  187.3 70.3 reduce-scatter.4
